TPU v7x, 512 devices: a whole 4x4x16 slice. The times are simulated.
512 devices in a mesh: sp: 32 (over z, core), tp: 16 (over y, x).
Axes of the slice: x: 4, y: 4, z: 16, core: 2. Of those that a mesh axis runs over, the one named last changes fastest.
Arguments:
- cotangent: bfloat16 [4096, 2048], P('sp'), may hold values from -6 to 6
- normed: bfloat16 [4096, 2048], P('sp'), may hold values from -6 to 6
- inverse_root_mean_square: float32 [4096], P('sp'), may hold values from 0.5 to 2
- expert_norm_scale: float32 [2048], replicated, may hold values from 0.1 to 1.9
- routes: int32 [4096, 2], P('sp'), may hold values from 0 to 31, all different within a row; in each aligned block of 128 rows (0 to 127, 128 to 255, ...) at most 16 rows name the same one
- route_probability_weight: float32 [4096, 2], P('sp'), may hold values from 0.2 to 1
- gate_weight: bfloat16 [32, 2048, 2048], P('sp', None, 'tp'), may hold values from -0.125 to 0.125
- up_weight: bfloat16 [32, 2048, 2048], P('sp', None, 'tp'), may hold values from -0.125 to 0.125
- down_weight: bfloat16 [32, 2048, 2048], P('sp', 'tp'), may hold values from -0.125 to 0.125
- recurrence_input: bfloat16 [4096, 1024], P('sp', 'tp'), may hold values from -6 to 6
- recurrence_gate_logits: bfloat16 [4096, 1024], P('sp', 'tp'), may hold values from -6 to 6
- input_gate_logits: bfloat16 [4096, 1024], P('sp', 'tp'), may hold values from -6 to 6
- channel_decay_weight: float32 [1024], P('tp'), may hold values from 3 to 20
- extra_log_decay: float32 [4096, 1024], P('sp', 'tp'), may hold values from -1 to 0
- output_matrix: bfloat16 [2048, 1024], P(None, 'tp'), may hold values from -0.1875 to 0.1875
Outputs:
- grad_gate: bfloat16 [32, 2048, 2048], P('sp', None, 'tp')
- grad_up: bfloat16 [32, 2048, 2048], P('sp', None, 'tp')
- grad_down: bfloat16 [32, 2048, 2048], P('sp', 'tp')
- grad_out_weight: float32 [2048, 1024], P('sp', 'tp')
- grad_rec_input: float32 [4096, 1024], P('sp', 'tp')
- grad_decay_gate: float32 [4096, 1024], P('sp', 'tp')
- grad_input_gate: float32 [4096, 1024], P('sp', 'tp')
Inputs may be any that keep to these rules, and one draw needn't show every extreme that they name: `routes`: each row names 2 different experts; among the rows of one device no expert is named more than 16 times.
All inputs are finite; a program needn't handle non-finite values.
Results may differ from a plain program's by a relative error of at most 0.025.
Values may be sent and summed in bfloat16 or wider, within the bound.
A program may use at most 64 MiB of HBM per device.

v0:
```python
import jax
import jax.numpy as jnp
from jax import lax
from jax.sharding import Mesh
from jax.sharding import PartitionSpec as P

TP = ("tp_0", "tp_1")


def side_by_side(arrays, axis, split_dim, concat_dim, along):
    both = jnp.concatenate(arrays, axis=along)
    filled, at, gathered = (
        lax.all_to_all(both, axis, split_axis=split_dim, concat_axis=concat_dim, tiled=True),
        0,
        [],
    )
    for a in arrays:
        gathered.append(lax.slice_in_dim(filled, at, at + a.shape[along], axis=along))
        at += a.shape[along]
    return tuple(gathered)


def in_blocks(value, dim, count):
    dims = value.shape
    parts = value.reshape(*dims[:dim], count, dims[dim] // count, *dims[dim + 1 :])
    return jnp.moveaxis(parts, dim, 0)


def sum_at_owner(value, axis, dim):
    parts = in_blocks(value, dim, lax.axis_size(axis))
    arrived = lax.all_to_all(parts, axis, split_axis=0, concat_axis=0, tiled=True)
    return arrived.astype(jnp.float32).sum(axis=0)


def over_axes(value, axes):
    for axis in axes:
        value = lax.psum(value, axis)
    return value


def in_order(parts, dim):
    parts = jnp.moveaxis(parts, 0, dim)
    dims = parts.shape
    return parts.reshape(*dims[:dim], dims[dim] * dims[dim + 1], *dims[dim + 2 :])


def sent_to_all(value, axis):
    count = lax.axis_size(axis)
    return lax.all_to_all(
        jnp.broadcast_to(value[None], (count, *value.shape)), axis, 0, 0, tiled=True
    )


def gathered_copies(value, axis, dim):
    return in_order(sent_to_all(value, axis), dim)


def gathered_once(value, axis):
    leaves = jax.tree.leaves(value)
    sequence = sorted(range(len(leaves)), key=lambda k: -leaves[k].size)
    width = (1, *leaves[sequence[0]].shape)[-1]
    lines = [
        jnp.pad(leaves[k].reshape(-1), (0, -leaves[k].size % width)).reshape(-1, width)
        for k in sequence
    ]
    both, at, found = (sent_to_all(jnp.concatenate(lines), axis), 0, {})
    for k, line in zip(sequence, lines):
        section = both[:, at : at + len(line)].reshape(len(both), -1)
        found[k] = section[:, : leaves[k].size].reshape(-1, *leaves[k].shape)
        at += len(line)
    numbers = iter(range(len(leaves)))
    return jax.tree.map(lambda _: found[next(numbers)], value)


def joined_by_halves(pieces, combine):
    while len(jax.tree.leaves(pieces)[0]) > 1:
        pieces = jax.vmap(combine)(
            *(jax.tree.map(lambda part: part[side::2], pieces) for side in (0, 1))
        )
    return jax.tree.map(lambda part: part[0], pieces)


def entering(value, axis, combine, identity, reverse):
    count, here = (lax.axis_size(axis), lax.axis_index(axis))
    passed = jnp.arange(count) > here if reverse else jnp.arange(count) < here

    def kept(part, zero, own):
        part = jnp.where(
            passed.reshape(-1, *(1 for _ in own.shape)), part, jnp.asarray(zero, own.dtype)
        )
        return part[::-1] if reverse else part

    pieces = gathered_once(value, axis)
    return joined_by_halves(jax.tree.map(kept, pieces, identity, value), combine)


def link(earlier, later):
    return (earlier[0] * later[0], later[0] * earlier[1] + later[1])


def shards(
    cotangent,
    normed,
    inverse_root_mean_square,
    expert_norm_scale,
    routes,
    route_probability_weight,
    gate_weight,
    up_weight,
    down_weight,
    recurrence_input,
    recurrence_gate_logits,
    input_gate_logits,
    channel_decay_weight,
    extra_log_decay,
    output_matrix,
):
    tok_rows, features = normed.shape
    groups = lax.axis_size("sp")
    picks = routes.shape[1]
    capacity = 2 * picks * tok_rows // groups
    rowdims = (((0,), (0,)), ((), ()))
    coldims = (((1,), (1,)), ((), ()))
    chosen = routes.reshape(-1)
    member = (chosen[:, None] == jnp.arange(groups, dtype=jnp.int32)[None, :]).astype(jnp.int32)
    ranking = jnp.sum((jnp.cumsum(member, axis=0) - member) * member, axis=1)
    landing = chosen * capacity + ranking
    scaled = (
        route_probability_weight[:, :, None] * cotangent[:, None, :].astype(jnp.float32)
    ).astype(jnp.bfloat16)
    scaled = scaled.reshape(tok_rows * picks, features)
    copies = jnp.repeat(normed, picks, axis=0)
    grad_send = jnp.zeros((groups * capacity, features), jnp.bfloat16).at[landing].set(scaled)
    token_send = jnp.zeros((groups * capacity, features), jnp.bfloat16).at[landing].set(copies)
    grad_recv, token_recv = side_by_side((grad_send, token_send), "sp", 0, 0, 1)
    gate_w = gate_weight[0]
    up_w = up_weight[0]
    down_w = down_weight[0]
    gate_pre = jnp.dot(token_recv, gate_w, preferred_element_type=jnp.float32)
    up_pre = jnp.dot(token_recv, up_w, preferred_element_type=jnp.float32)
    sigma = jax.nn.sigmoid(gate_pre)
    swish = gate_pre * sigma
    active = (swish * up_pre).astype(jnp.bfloat16)
    d_active = lax.dot_general(grad_recv, down_w, coldims, preferred_element_type=jnp.float32)
    d_gate = (d_active * up_pre * sigma * (1.0 + gate_pre * (1.0 - sigma))).astype(jnp.bfloat16)
    d_up = (d_active * swish).astype(jnp.bfloat16)
    grad_down = lax.dot_general(
        active, grad_recv, rowdims, preferred_element_type=jnp.float32
    ).astype(jnp.bfloat16)
    grad_gate = lax.dot_general(
        token_recv, d_gate, rowdims, preferred_element_type=jnp.float32
    ).astype(jnp.bfloat16)
    grad_up = lax.dot_general(token_recv, d_up, rowdims, preferred_element_type=jnp.float32).astype(
        jnp.bfloat16
    )
    partial_rows = lax.dot_general(d_gate, gate_w, coldims, preferred_element_type=jnp.float32)
    partial_rows = partial_rows + lax.dot_general(
        d_up, up_w, coldims, preferred_element_type=jnp.float32
    )
    shared = sum_at_owner(partial_rows.astype(jnp.bfloat16), TP, 1).astype(jnp.bfloat16)
    returned = lax.all_to_all(shared, "sp", split_axis=0, concat_axis=0, tiled=True)
    slice_width = returned.shape[1]
    offset = lax.axis_index(TP) * slice_width
    gain_part = lax.dynamic_slice_in_dim(expert_norm_scale, offset, slice_width, 0)
    normed_part = lax.dynamic_slice_in_dim(normed, offset, slice_width, 1)
    cot_part = lax.dynamic_slice_in_dim(cotangent, offset, slice_width, 1)
    d_norm = jnp.sum(
        returned[landing].astype(jnp.float32).reshape(tok_rows, picks, slice_width), axis=1
    )
    nhat = normed_part.astype(jnp.float32) / gain_part[None, :]
    gained = gain_part[None, :] * d_norm
    stat = over_axes(jnp.sum(gained * nhat, axis=1), TP)[:, None] / features
    mix_part = (
        cot_part.astype(jnp.float32) + inverse_root_mean_square[:, None] * (gained - nhat * stat)
    ).astype(jnp.bfloat16)
    d_mix = gathered_copies(mix_part, TP, 1)
    retention_factor = jax.nn.sigmoid(recurrence_gate_logits.astype(jnp.float32))
    admit = jax.nn.sigmoid(input_gate_logits.astype(jnp.float32))
    signal = recurrence_input.astype(jnp.float32)
    decay_speed = jax.nn.softplus(-channel_decay_weight)
    log_retention = -8.0 * retention_factor * decay_speed[None, :] + extra_log_decay
    keep = jnp.exp(log_retention)
    scale_in = jnp.sqrt(-jnp.expm1(2.0 * log_retention))
    driven = scale_in * admit * signal
    channels = keep.shape[1]
    identity = (jnp.ones((channels,), jnp.float32), jnp.zeros((channels,), jnp.float32))
    keep_cum, state_loc = lax.associative_scan(link, (keep, driven), axis=0)
    _, state_in = entering((keep_cum[-1], state_loc[-1]), "sp", link, identity, False)
    state = state_loc + keep_cum * state_in[None, :]
    hidden = state.astype(jnp.bfloat16)
    state_prev = jnp.concatenate([state_in[None, :], state[:-1]], axis=0)
    grad_out_weight = sum_at_owner(
        lax.dot_general(d_mix, hidden, rowdims, preferred_element_type=jnp.float32).astype(
            jnp.bfloat16
        ),
        "sp",
        0,
    )
    d_state = jnp.dot(d_mix, output_matrix, preferred_element_type=jnp.float32)
    keep_next = jnp.concatenate([keep[1:], jnp.ones((1, channels), jnp.float32)], axis=0)
    tail_keep, grad_loc = lax.associative_scan(link, (keep_next, d_state), reverse=True, axis=0)
    block_map = (keep[0] * tail_keep[0], keep[0] * grad_loc[0])
    _, grad_enter = entering(block_map, "sp", link, identity, True)
    total = grad_loc + tail_keep * grad_enter[None, :]
    grad_rec_input = total * scale_in * admit
    grad_input_gate = total * scale_in * signal * admit * (1.0 - admit)
    d_log = total * state_prev * keep - total * admit * signal * keep * keep / scale_in
    grad_decay_gate = (
        d_log * (-8.0 * decay_speed[None, :]) * retention_factor * (1.0 - retention_factor)
    )
    return (
        grad_gate[None],
        grad_up[None],
        grad_down[None],
        grad_out_weight,
        grad_rec_input,
        grad_decay_gate,
        grad_input_gate,
    )


def solution(mesh):
    finer = Mesh(mesh.devices.reshape(mesh.shape["sp"], 4, 4), ("sp", "tp_0", "tp_1"))
    placed = (
        P("sp", None),
        P("sp", None),
        P("sp"),
        P(),
        P("sp", None),
        P("sp", None),
        P("sp", None, TP),
        P("sp", None, TP),
        P("sp", TP, None),
        P("sp", TP),
        P("sp", TP),
        P("sp", TP),
        P(TP),
        P("sp", TP),
        P(None, TP),
    )
    return jax.shard_map(
        shards,
        mesh=finer,
        in_specs=placed,
        out_specs=(
            P("sp", None, TP),
            P("sp", None, TP),
            P("sp", TP, None),
            P("sp", TP),
            P("sp", TP),
            P("sp", TP),
            P("sp", TP),
        ),
        check_vma=False,
    )
```

profile of v0, /device:TPU:1, one launch (start us, length us, event | category | flops | bytes accessed | tf_op | source)
XLA Modules:
  0.0 428.7 jit_solution(14606756271678646964)
XLA Ops:
  0.7 0.8 broadcast_multiply_fusion
  1.4 0.8 copy.99
  3.6 1.7 broadcast_in_dim.73
  5.3 1.2 reshape.155
  6.5 2.4 mul.410
  8.9 2.7 mul.411
  12.0 4.4 %scatter_custom_fusion.1 = bf16[512,2048]{1,0:T(8,128)(2,1)} fusion(s32[256]{0:T(256)S(1)} %bitcast.130, bf16[256,2048]{1,0:T(8,128)(2,1)} %reshape.155, bf16[]{:T(256)} %constant.16.clone.1), kind=kCustom, calls=%fused_computation.27 | custom fusion | bytes 2097664 | tf_op jit(solution)/shard_map/scatter | solution.py:134
  16.4 3.8 scatter_custom_fusion
  20.2 2.7 pad_maximum_fusion
  22.9 207.4 %all_to_all.49 = bf16[32,16,4096]{2,1,0:T(8,128)(2,1)S(1)} all-to-all(bf16[32,16,4096]{2,1,0:T(8,128)(2,1)S(1)} %bitcast.99), channel_id=1, replica_groups=mesh['sp'=32,'tp_0'=4,'tp_1'=4] {'sp'}, dimensions={0} | all-to-all | bytes 8388608 | tf_op jit(solution)/shard_map/all_to_all | solution.py:13
  235.7 34.0 %all_to_all.50 = bf16[16,512,128]{2,1,0:T(8,128)(2,1)S(1)} all-to-all(bf16[16,512,128]{2,1,0:T(8,128)(2,1)S(1)} %bitcast.100), channel_id=1, replica_groups=mesh['sp'=32,'tp_0'=4,'tp_1'=4] {'tp_0','tp_1'}, dimensions={0} | all-to-all | bytes 4194304 | tf_op jit(solution)/shard_map/all_to_all | solution.py:31
  269.7 1.0 reduce_sum.52
  270.7 5.5 %all-to-all-start.2 = ((bf16[32,16,128]{2,1,0:T(8,128)(2,1)}), bf16[32,16,128]{2,1,0:T(8,128)(2,1)S(1)}, u32[]{:S(2)}, u32[]{:S(2)}) async-start(bf16[32,16,128]{2,1,0:T(8,128)(2,1)} %bitcast.12), calls=%async_computation.2 | async-start | bytes 262144 | tf_op jit(solution)/shard_map/all_to_all | solution.py:161
  276.2 0.8 dynamic_slice.10
  277.0 15.4 %all-to-all-done.2 = bf16[32,16,128]{2,1,0:T(8,128)(2,1)S(1)} async-done(((bf16[32,16,128]{2,1,0:T(8,128)(2,1)}), bf16[32,16,128]{2,1,0:T(8,128)(2,1)S(1)}, u32[]{:S(2)}, u32[]{:S(2)}) %all-to-all-start.2) | async-done | bytes 131104 | tf_op jit(solution)/shard_map/all_to_all | solution.py:161
  292.4 0.9 gather_fusion
  293.5 0.9 multiply_reduce_fusion
  294.3 6.6 %psum.14 = f32[128]{0:T(128)S(1)} all-reduce(f32[128]{0:T(128)S(1)} %multiply_reduce_fusion), channel_id=1, replica_groups=mesh['sp'=32,'tp_0'=4,'tp_1'=4] {'tp_0'}, use_global_device_ids=true, to_apply=%region_8.9 | all-reduce | flops 128 | bytes 1024 | tf_op jit(solution)/shard_map/psum | solution.py:37
  300.9 6.7 %psum.15 = f32[128]{0:T(128)S(1)} all-reduce(f32[128]{0:T(128)S(1)} %psum.14), channel_id=1, replica_groups=mesh['sp'=32,'tp_0'=4,'tp_1'=4] {'tp_1'}, use_global_device_ids=true, to_apply=%region_9.10 | all-reduce | flops 128 | bytes 1024 | tf_op jit(solution)/shard_map/psum | solution.py:37
  307.6 0.9 add_convert_fusion.1
  308.6 0.9 broadcast_in_dim.77
  309.5 4.1 all-to-all-start.3
  317.8 4.8 %all-to-all-done.3 = bf16[16,128,128]{1,2,0:T(8,128)(2,1)S(1)} async-done(((bf16[16,128,128]{1,2,0:T(8,128)(2,1)}), bf16[16,128,128]{1,2,0:T(8,128)(2,1)S(1)}, u32[]{:S(2)}, u32[]{:S(2)}) %all-to-all-start.3) | async-done | bytes 524320 | tf_op jit(solution)/shard_map/all_to_all | solution.py:49
  338.4 10.1 %all-to-all-start.6 = ((f32[32,1,128]{2,1,0:T(1,128)}), f32[32,1,128]{2,1,0:T(1,128)S(1)}, u32[]{:S(2)}, u32[]{:S(2)}) async-start(f32[32,1,128]{2,1,0:T(1,128)} %reshape.170), calls=%async_computation.6 | async-start | bytes 32768 | tf_op jit(solution)/shard_map/all_to_all | solution.py:49
  348.7 11.5 %all-to-all-done.6 = f32[32,1,128]{2,1,0:T(1,128)S(1)} async-done(((f32[32,1,128]{2,1,0:T(1,128)}), f32[32,1,128]{2,1,0:T(1,128)S(1)}, u32[]{:S(2)}, u32[]{:S(2)}) %all-to-all-start.6) | async-done | bytes 16416 | tf_op jit(solution)/shard_map/all_to_all | solution.py:49
  380.0 15.4 %all_to_all.51 = f32[32,1,128]{2,1,0:T(1,128)S(1)} all-to-all(f32[32,1,128]{2,1,0:T(1,128)S(1)} %reshape.166), channel_id=1, replica_groups=mesh['sp'=32,'tp_0'=4,'tp_1'=4] {'sp'}, dimensions={0} | all-to-all | bytes 32768 | tf_op jit(solution)/shard_map/all_to_all | solution.py:49
  400.0 1.1 reshape.168
  401.1 4.7 %all-to-all-start.5 = ((bf16[32,2,2048]{2,1,0:T(2,128)(2,1)}), bf16[32,2,2048]{2,1,0:T(2,128)(2,1)S(1)}, u32[]{:S(2)}, u32[]{:S(2)}) async-start(bf16[32,2,2048]{2,1,0:T(2,128)(2,1)} %reshape.168), calls=%async_computation.5 | async-start | bytes 524288 | tf_op jit(solution)/shard_map/all_to_all | solution.py:31
  405.8 3.3 fusion
  409.1 3.2 fusion.1
  412.3 1.3 fusion.2
  414.3 13.0 %all-to-all-done.5 = bf16[32,2,2048]{2,1,0:T(2,128)(2,1)S(1)} async-done(((bf16[32,2,2048]{2,1,0:T(2,128)(2,1)}), bf16[32,2,2048]{2,1,0:T(2,128)(2,1)S(1)}, u32[]{:S(2)}, u32[]{:S(2)}) %all-to-all-start.5) | async-done | bytes 262176 | tf_op jit(solution)/shard_map/all_to_all | solution.py:31
  (345 shorter events, 52.2 us)
Async XLA Ops:
  0.6 229.6 %copy-start = (bf16[1,2048,128]{2,1,0:T(8,128)(2,1)S(1)}, bf16[1,2048,128]{2,1,0:T(8,128)(2,1)}, u32[]{:S(2)}) copy-start(bf16[1,2048,128]{2,1,0:T(8,128)(2,1)} %param.21) | copy-start | bytes 1572868
  0.6 5.9 %copy-start.3 = (bf16[128,2048]{1,0:T(8,128)(2,1)S(1)}, bf16[128,2048]{1,0:T(8,128)(2,1)}, u32[]{:S(2)}) copy-start(bf16[128,2048]{1,0:T(8,128)(2,1)} %param.15) | copy-start | bytes 1572868
  8.9 2.7 copy-start.10
  230.2 2.1 copy-start.1
  230.2 1.4 copy-start.4
  231.6 2.0 copy-start.14
  231.6 1.3 copy-start.12
  233.0 0.7 copy-start.16
  269.7 37.9 %copy-start.11 = (f32[128]{0:T(128)S(1)}, f32[128]{0:T(128)}, u32[]{:S(2)}) copy-start(f32[128]{0:T(128)} %param.17) | copy-start | bytes 1540
  269.7 43.9 %copy-start.13 = (f32[64]{0:T(128)S(1)}, f32[64]{0:T(128)}, u32[]{:S(2)}) copy-start(f32[64]{0:T(128)} %param.27) | copy-start | bytes 772
  269.7 44.0 %copy-start.5 = (f32[128,64]{0,1:T(8,128)S(1)}, f32[128,64]{0,1:T(8,128)}, u32[]{:S(2)}) copy-start(f32[128,64]{0,1:T(8,128)} %param.28) | copy-start | bytes 98308
  269.7 44.0 %copy-start.7 = (bf16[128,64]{0,1:T(8,128)(2,1)S(1)}, bf16[128,64]{0,1:T(8,128)(2,1)}, u32[]{:S(2)}) copy-start(bf16[128,64]{0,1:T(8,128)(2,1)} %param.25) | copy-start | bytes 49156
  270.7 51.9 %copy-start.6 = (bf16[2048,64]{0,1:T(8,128)(2,1)S(1)}, bf16[2048,64]{0,1:T(8,128)(2,1)}, u32[]{:S(2)}) copy-start(bf16[2048,64]{0,1:T(8,128)(2,1)} %param.29) | copy-start | bytes 786436
  270.7 21.7 %all-to-all-start.2 = ((bf16[32,16,128]{2,1,0:T(8,128)(2,1)}), bf16[32,16,128]{2,1,0:T(8,128)(2,1)S(1)}, u32[]{:S(2)}, u32[]{:S(2)}) async-start(bf16[32,16,128]{2,1,0:T(8,128)(2,1)} %bitcast.12), calls=%async_computation.2 | async-start | bytes 262144 | tf_op jit(solution)/shard_map/all_to_all | solution.py:161
  309.5 13.1 %all-to-all-start.3 = ((bf16[16,128,128]{1,2,0:T(8,128)(2,1)}), bf16[16,128,128]{1,2,0:T(8,128)(2,1)S(1)}, u32[]{:S(2)}, u32[]{:S(2)}) async-start(bf16[16,128,128]{1,2,0:T(8,128)(2,1)} %broadcast_in_dim.77), calls=%async_computation.3 | async-start | bytes 1048576 | tf_op jit(solution)/shard_map/all_to_all | solution.py:49
  334.7 29.7 %copy-start.8 = (bf16[128,64]{0,1:T(8,128)(2,1)S(1)}, bf16[128,64]{0,1:T(8,128)(2,1)}, u32[]{:S(2)}) copy-start(bf16[128,64]{0,1:T(8,128)(2,1)} %param.24) | copy-start | bytes 49156
  334.7 29.7 %copy-start.9 = (bf16[128,64]{0,1:T(8,128)(2,1)S(1)}, bf16[128,64]{0,1:T(8,128)(2,1)}, u32[]{:S(2)}) copy-start(bf16[128,64]{0,1:T(8,128)(2,1)} %param.26) | copy-start | bytes 49156
  338.4 21.9 %all-to-all-start.6 = ((f32[32,1,128]{2,1,0:T(1,128)}), f32[32,1,128]{2,1,0:T(1,128)S(1)}, u32[]{:S(2)}, u32[]{:S(2)}) async-start(f32[32,1,128]{2,1,0:T(1,128)} %reshape.170), calls=%async_computation.6 | async-start | bytes 32768 | tf_op jit(solution)/shard_map/all_to_all | solution.py:49
  401.1 26.2 %all-to-all-start.5 = ((bf16[32,2,2048]{2,1,0:T(2,128)(2,1)}), bf16[32,2,2048]{2,1,0:T(2,128)(2,1)S(1)}, u32[]{:S(2)}, u32[]{:S(2)}) async-start(bf16[32,2,2048]{2,1,0:T(2,128)(2,1)} %reshape.168), calls=%async_computation.5 | async-start | bytes 524288 | tf_op jit(solution)/shard_map/all_to_all | solution.py:31
  405.8 6.5 %copy-start.2 = (bf16[32,16,4096]{2,1,0:T(8,128)(2,1)S(1)}, bf16[32,16,4096]{2,1,0:T(8,128)(2,1)}, u32[]{:S(2)}) copy-start(bf16[32,16,4096]{2,1,0:T(8,128)(2,1)} %copy-done.1) | copy-start | bytes 12582916
  409.1 3.2 copy-start.15
  409.1 3.2 copy-start.17
where the time goes:
time: 436 us; the launch traced here: 429 us
  blocking collectives  270 us (62%)
  local copies, waits for them, and re-layouts  57.2 us (13%)
  waiting for transfers between devices  44.7 us (10%)
  starting transfers between devices  24.5 us (6%)
  other arithmetic  17.6 us (4%)
  matrix products  11.9 us (3%)
    all_to_all x1, blocking collectives, side_by_side(): lax.all_to_all(both, axis, split_axis=split_dim, concat_axis=concat_dim,...  207 us
    all_to_all x1, blocking collectives, sum_at_owner(): lax.all_to_all(parts, axis, split_axis=0, concat_axis=0, tiled=True)  34 us
    all_to_all x2, waiting for transfers between devices, sent_to_all(): lax.all_to_all(jnp.broadcast_to(value[None], (count, *value.shape)), axis...  16.4 us
    all_to_all x1, waiting for transfers between devices, shards(): lax.all_to_all(shared, 'sp', split_axis=0, concat_axis=0, tiled=True)  15.4 us
    all_to_all x1, blocking collectives, sent_to_all(): lax.all_to_all(jnp.broadcast_to(value[None], (count, *value.shape)), axis...  15.4 us
    all_to_all x2, starting transfers between devices, sent_to_all(): lax.all_to_all(jnp.broadcast_to(value[None], (count, *value.shape)), axis...  14.2 us
    psum x2, blocking collectives, over_axes(): value = lax.psum(value, axis)  13.3 us
    all_to_all x1, waiting for transfers between devices, sum_at_owner(): lax.all_to_all(parts, axis, split_axis=0, concat_axis=0, tiled=True)  13 us
  transfers between devices with their start and end apart: 4, of which 4 were waited for; matrix products, arithmetic and copies ran while one was open for 3% of the time, Pallas kernels for 0%

commit v1 on v0

--- a/solution.py
+++ b/solution.py
@@ -34,7 +34,8 @@
 
 def over_axes(value, axes):
     for axis in axes:
-        value = lax.psum(value, axis)
+        cells = lax.all_gather(value, axis, axis=0, tiled=False)
+        value = cells.sum(axis=0)
     return value
 
 

time: 436 us -> 435 us (level)
    psum x2 -> x0, blocking collectives: 13.3 us -> none  [over_axes(): value = lax.psum(value, axis)]
    all_gather x0 -> x2, blocking collectives: none -> 11.6 us  [over_axes(): cells = lax.all_gather(value, axis, axis=0, tiled=False)]
where the time goes in v1:
time: 435 us; the launch traced here: 427 us
  blocking collectives  268 us (62%)
  local copies, waits for them, and re-layouts  57.2 us (13%)
  waiting for transfers between devices  44.8 us (10%)
  starting transfers between devices  24.7 us (6%)
  other arithmetic  17.7 us (4%)
  matrix products  11.9 us (3%)
    all_to_all x1, blocking collectives, side_by_side(): lax.all_to_all(both, axis, split_axis=split_dim, concat_axis=concat_dim,...  207 us
    all_to_all x1, blocking collectives, sum_at_owner(): lax.all_to_all(parts, axis, split_axis=0, concat_axis=0, tiled=True)  34 us
    all_to_all x2, waiting for transfers between devices, sent_to_all(): lax.all_to_all(jnp.broadcast_to(value[None], (count, *value.shape)), axis...  16.4 us
    all_to_all x1, waiting for transfers between devices, shards(): lax.all_to_all(shared, 'sp', split_axis=0, concat_axis=0, tiled=True)  15.4 us
    all_to_all x1, blocking collectives, sent_to_all(): lax.all_to_all(jnp.broadcast_to(value[None], (count, *value.shape)), axis...  15.4 us
    all_to_all x2, starting transfers between devices, sent_to_all(): lax.all_to_all(jnp.broadcast_to(value[None], (count, *value.shape)), axis...  14.4 us
    all_to_all x1, waiting for transfers between devices, sum_at_owner(): lax.all_to_all(parts, axis, split_axis=0, concat_axis=0, tiled=True)  13 us
    all_gather x2, blocking collectives, over_axes(): cells = lax.all_gather(value, axis, axis=0, tiled=False)  11.6 us
  transfers between devices with their start and end apart: 4, of which 4 were waited for; matrix products, arithmetic and copies ran while one was open for 3% of the time, Pallas kernels for 0%

profile of v1, /device:TPU:1, one launch (start us, length us, event | category | flops | bytes accessed | tf_op | source)
XLA Modules:
  0.0 427.2 jit_solution(8712252438477142159)
XLA Ops:
  0.7 0.8 broadcast_multiply_fusion
  1.4 0.8 copy.99
  3.6 1.7 broadcast_in_dim.73
  5.3 1.2 reshape.157
  6.5 2.4 mul.410
  8.9 2.7 mul.411
  12.0 4.4 %scatter_custom_fusion.1 = bf16[512,2048]{1,0:T(8,128)(2,1)} fusion(s32[256]{0:T(256)S(1)} %bitcast.132, bf16[256,2048]{1,0:T(8,128)(2,1)} %reshape.157, bf16[]{:T(256)} %constant.16.clone.1), kind=kCustom, calls=%fused_computation.27 | custom fusion | bytes 2097664 | tf_op jit(solution)/shard_map/scatter | solution.py:135
  16.4 3.8 scatter_custom_fusion
  20.2 2.7 pad_maximum_fusion
  22.9 207.4 %all_to_all.49 = bf16[32,16,4096]{2,1,0:T(8,128)(2,1)S(1)} all-to-all(bf16[32,16,4096]{2,1,0:T(8,128)(2,1)S(1)} %bitcast.101), channel_id=1, replica_groups=mesh['sp'=32,'tp_0'=4,'tp_1'=4] {'sp'}, dimensions={0} | all-to-all | bytes 8388608 | tf_op jit(solution)/shard_map/all_to_all | solution.py:13
  235.7 34.0 %all_to_all.50 = bf16[16,512,128]{2,1,0:T(8,128)(2,1)S(1)} all-to-all(bf16[16,512,128]{2,1,0:T(8,128)(2,1)S(1)} %bitcast.102), channel_id=1, replica_groups=mesh['sp'=32,'tp_0'=4,'tp_1'=4] {'tp_0','tp_1'}, dimensions={0} | all-to-all | bytes 4194304 | tf_op jit(solution)/shard_map/all_to_all | solution.py:31
  269.7 1.0 reduce_sum.70
  270.7 5.5 %all-to-all-start.2 = ((bf16[32,16,128]{2,1,0:T(8,128)(2,1)}), bf16[32,16,128]{2,1,0:T(8,128)(2,1)S(1)}, u32[]{:S(2)}, u32[]{:S(2)}) async-start(bf16[32,16,128]{2,1,0:T(8,128)(2,1)} %bitcast.12), calls=%async_computation.2 | async-start | bytes 262144 | tf_op jit(solution)/shard_map/all_to_all | solution.py:162
  276.2 0.8 dynamic_slice.10
  277.0 15.4 %all-to-all-done.2 = bf16[32,16,128]{2,1,0:T(8,128)(2,1)S(1)} async-done(((bf16[32,16,128]{2,1,0:T(8,128)(2,1)}), bf16[32,16,128]{2,1,0:T(8,128)(2,1)S(1)}, u32[]{:S(2)}, u32[]{:S(2)}) %all-to-all-start.2) | async-done | bytes 131104 | tf_op jit(solution)/shard_map/all_to_all | solution.py:162
  292.4 0.9 gather_fusion
  293.5 0.9 multiply_reduce_fusion
  294.3 5.8 %all-gather.2 = f32[4,1,128]{2,1,0:T(1,128)S(1)} all-gather(f32[1,1,128]{2,1,0:T(1,128)S(1)} %bitcast.136), channel_id=2, replica_groups=mesh['sp'=32,'tp_0'=4,'tp_1'=4] {'tp_0'}, dimensions={0}, use_global_device_ids=true | all-gather | bytes 2560 | tf_op jit(solution)/shard_map/all_gather | solution.py:37
  300.2 5.8 %all-gather.3 = f32[4,1,128]{2,1,0:T(1,128)S(1)} all-gather(f32[1,1,128]{2,1,0:T(1,128)S(1)} %bitcast.137), channel_id=3, replica_groups=mesh['sp'=32,'tp_0'=4,'tp_1'=4] {'tp_1'}, dimensions={0}, use_global_device_ids=true | all-gather | bytes 2560 | tf_op jit(solution)/shard_map/all_gather | solution.py:37
  306.0 0.9 add_convert_fusion.1
  307.0 0.9 broadcast_in_dim.77
  307.9 4.1 all-to-all-start.3
  316.1 4.8 %all-to-all-done.3 = bf16[16,128,128]{1,2,0:T(8,128)(2,1)S(1)} async-done(((bf16[16,128,128]{1,2,0:T(8,128)(2,1)}), bf16[16,128,128]{1,2,0:T(8,128)(2,1)S(1)}, u32[]{:S(2)}, u32[]{:S(2)}) %all-to-all-start.3) | async-done | bytes 524320 | tf_op jit(solution)/shard_map/all_to_all | solution.py:50
  336.8 10.3 %all-to-all-start.6 = ((f32[32,1,128]{2,1,0:T(1,128)}), f32[32,1,128]{2,1,0:T(1,128)S(1)}, u32[]{:S(2)}, u32[]{:S(2)}) async-start(f32[32,1,128]{2,1,0:T(1,128)} %reshape.180), calls=%async_computation.6 | async-start | bytes 32768 | tf_op jit(solution)/shard_map/all_to_all | solution.py:50
  347.2 11.5 %all-to-all-done.6 = f32[32,1,128]{2,1,0:T(1,128)S(1)} async-done(((f32[32,1,128]{2,1,0:T(1,128)}), f32[32,1,128]{2,1,0:T(1,128)S(1)}, u32[]{:S(2)}, u32[]{:S(2)}) %all-to-all-start.6) | async-done | bytes 16416 | tf_op jit(solution)/shard_map/all_to_all | solution.py:50
  378.6 15.4 %all_to_all.51 = f32[32,1,128]{2,1,0:T(1,128)S(1)} all-to-all(f32[32,1,128]{2,1,0:T(1,128)S(1)} %reshape.176), channel_id=1, replica_groups=mesh['sp'=32,'tp_0'=4,'tp_1'=4] {'sp'}, dimensions={0} | all-to-all | bytes 32768 | tf_op jit(solution)/shard_map/all_to_all | solution.py:50
  398.5 1.1 reshape.178
  399.6 4.7 %all-to-all-start.5 = ((bf16[32,2,2048]{2,1,0:T(2,128)(2,1)}), bf16[32,2,2048]{2,1,0:T(2,128)(2,1)S(1)}, u32[]{:S(2)}, u32[]{:S(2)}) async-start(bf16[32,2,2048]{2,1,0:T(2,128)(2,1)} %reshape.178), calls=%async_computation.5 | async-start | bytes 524288 | tf_op jit(solution)/shard_map/all_to_all | solution.py:31
  404.3 3.3 fusion
  407.6 3.2 fusion.1
  410.9 1.3 fusion.2
  412.9 13.0 %all-to-all-done.5 = bf16[32,2,2048]{2,1,0:T(2,128)(2,1)S(1)} async-done(((bf16[32,2,2048]{2,1,0:T(2,128)(2,1)}), bf16[32,2,2048]{2,1,0:T(2,128)(2,1)S(1)}, u32[]{:S(2)}, u32[]{:S(2)}) %all-to-all-start.5) | async-done | bytes 262176 | tf_op jit(solution)/shard_map/all_to_all | solution.py:31
  (347 shorter events, 52.2 us)
Async XLA Ops:
  0.6 229.6 %copy-start = (bf16[1,2048,128]{2,1,0:T(8,128)(2,1)S(1)}, bf16[1,2048,128]{2,1,0:T(8,128)(2,1)}, u32[]{:S(2)}) copy-start(bf16[1,2048,128]{2,1,0:T(8,128)(2,1)} %param.21) | copy-start | bytes 1572868
  0.6 5.9 %copy-start.3 = (bf16[128,2048]{1,0:T(8,128)(2,1)S(1)}, bf16[128,2048]{1,0:T(8,128)(2,1)}, u32[]{:S(2)}) copy-start(bf16[128,2048]{1,0:T(8,128)(2,1)} %param.15) | copy-start | bytes 1572868
  8.9 2.7 copy-start.10
  230.2 2.1 copy-start.1
  230.2 1.4 copy-start.4
  231.6 2.0 copy-start.14
  231.6 1.3 copy-start.12
  233.0 0.7 copy-start.16
  269.7 36.3 %copy-start.11 = (f32[128]{0:T(128)S(1)}, f32[128]{0:T(128)}, u32[]{:S(2)}) copy-start(f32[128]{0:T(128)} %param.17) | copy-start | bytes 1540
  269.7 42.3 %copy-start.13 = (f32[64]{0:T(128)S(1)}, f32[64]{0:T(128)}, u32[]{:S(2)}) copy-start(f32[64]{0:T(128)} %param.27) | copy-start | bytes 772
  269.7 42.4 %copy-start.5 = (f32[128,64]{0,1:T(8,128)S(1)}, f32[128,64]{0,1:T(8,128)}, u32[]{:S(2)}) copy-start(f32[128,64]{0,1:T(8,128)} %param.28) | copy-start | bytes 98308
  269.7 42.4 %copy-start.7 = (bf16[128,64]{0,1:T(8,128)(2,1)S(1)}, bf16[128,64]{0,1:T(8,128)(2,1)}, u32[]{:S(2)}) copy-start(bf16[128,64]{0,1:T(8,128)(2,1)} %param.25) | copy-start | bytes 49156
  270.7 50.3 %copy-start.6 = (bf16[2048,64]{0,1:T(8,128)(2,1)S(1)}, bf16[2048,64]{0,1:T(8,128)(2,1)}, u32[]{:S(2)}) copy-start(bf16[2048,64]{0,1:T(8,128)(2,1)} %param.29) | copy-start | bytes 786436
  270.7 21.7 %all-to-all-start.2 = ((bf16[32,16,128]{2,1,0:T(8,128)(2,1)}), bf16[32,16,128]{2,1,0:T(8,128)(2,1)S(1)}, u32[]{:S(2)}, u32[]{:S(2)}) async-start(bf16[32,16,128]{2,1,0:T(8,128)(2,1)} %bitcast.12), calls=%async_computation.2 | async-start | bytes 262144 | tf_op jit(solution)/shard_map/all_to_all | solution.py:162
  307.9 13.1 %all-to-all-start.3 = ((bf16[16,128,128]{1,2,0:T(8,128)(2,1)}), bf16[16,128,128]{1,2,0:T(8,128)(2,1)S(1)}, u32[]{:S(2)}, u32[]{:S(2)}) async-start(bf16[16,128,128]{1,2,0:T(8,128)(2,1)} %broadcast_in_dim.77), calls=%async_computation.3 | async-start | bytes 1048576 | tf_op jit(solution)/shard_map/all_to_all | solution.py:50
  333.1 29.9 %copy-start.8 = (bf16[128,64]{0,1:T(8,128)(2,1)S(1)}, bf16[128,64]{0,1:T(8,128)(2,1)}, u32[]{:S(2)}) copy-start(bf16[128,64]{0,1:T(8,128)(2,1)} %param.24) | copy-start | bytes 49156
  333.1 29.9 %copy-start.9 = (bf16[128,64]{0,1:T(8,128)(2,1)S(1)}, bf16[128,64]{0,1:T(8,128)(2,1)}, u32[]{:S(2)}) copy-start(bf16[128,64]{0,1:T(8,128)(2,1)} %param.26) | copy-start | bytes 49156
  336.8 22.0 %all-to-all-start.6 = ((f32[32,1,128]{2,1,0:T(1,128)}), f32[32,1,128]{2,1,0:T(1,128)S(1)}, u32[]{:S(2)}, u32[]{:S(2)}) async-start(f32[32,1,128]{2,1,0:T(1,128)} %reshape.180), calls=%async_computation.6 | async-start | bytes 32768 | tf_op jit(solution)/shard_map/all_to_all | solution.py:50
  399.6 26.3 %all-to-all-start.5 = ((bf16[32,2,2048]{2,1,0:T(2,128)(2,1)}), bf16[32,2,2048]{2,1,0:T(2,128)(2,1)S(1)}, u32[]{:S(2)}, u32[]{:S(2)}) async-start(bf16[32,2,2048]{2,1,0:T(2,128)(2,1)} %reshape.178), calls=%async_computation.5 | async-start | bytes 524288 | tf_op jit(solution)/shard_map/all_to_all | solution.py:31
  404.3 6.5 %copy-start.2 = (bf16[32,16,4096]{2,1,0:T(8,128)(2,1)S(1)}, bf16[32,16,4096]{2,1,0:T(8,128)(2,1)}, u32[]{:S(2)}) copy-start(bf16[32,16,4096]{2,1,0:T(8,128)(2,1)} %copy-done.1) | copy-start | bytes 12582916
  407.6 3.2 copy-start.15
  407.6 3.2 copy-start.17
